TPU v7x, 32 devices: a whole 2x2x4 slice. The times are simulated.
32 devices in a mesh: ep: 16 (over z, y, x), tp: 2 (over core).
Axes of the slice: x: 2, y: 2, z: 4, core: 2. Of those that a mesh axis runs over, the one named last changes fastest.
Arguments:
- tokens: bfloat16 [256, 2048], P('ep'), may hold values from -6 to 6
- lengths: int32 [256], P('ep'), may hold values from 1024 to 8191
- prior_state: float32 [256, 16, 64, 64], P('ep', 'tp'), may hold values from -2 to 2
- mix_gain: float32 [2048], replicated, may hold values from 0.1 to 1.9
- post_gain: float32 [2048], replicated, may hold values from 0.1 to 1.9
- ffn_gain: float32 [2048], replicated, may hold values from 0.1 to 1.9
- out_gain: float32 [2048], replicated, may hold values from 0.1 to 1.9
- query_weight: bfloat16 [2048, 1024], P('ep', 'tp'), may hold values from -0.125 to 0.125
- key_weight: bfloat16 [2048, 1024], P('ep', 'tp'), may hold values from -0.125 to 0.125
- value_weight: bfloat16 [2048, 1024], P('ep', 'tp'), may hold values from -0.125 to 0.125
- gate_weight: bfloat16 [2048, 1024], P('ep', 'tp'), may hold values from -0.125 to 0.125
- out_weight: bfloat16 [1024, 2048], P('tp', 'ep'), may hold values from -0.1875 to 0.1875
- routes: int32 [256, 6], P('ep'), may hold values from 0 to 15, all different within a row; in each aligned block of 16 rows (0 to 15, 16 to 31, ...) at most 8 rows name the same one
- route_gates: float32 [256, 6], P('ep'), may hold values from 0.1 to 0.9
- expert_gate: bfloat16 [16, 2048, 512], P('ep', None, 'tp'), may hold values from -0.125 to 0.125
- expert_up: bfloat16 [16, 2048, 512], P('ep', None, 'tp'), may hold values from -0.125 to 0.125
- expert_down: bfloat16 [16, 512, 2048], P('ep', 'tp'), may hold values from -0.25 to 0.25
- shared_gate: bfloat16 [2048, 512], P(None, 'tp'), may hold values from -0.125 to 0.125
- shared_up: bfloat16 [2048, 512], P(None, 'tp'), may hold values from -0.125 to 0.125
- shared_down: bfloat16 [512, 2048], P('tp'), may hold values from -0.25 to 0.25
Outputs:
- result: bfloat16 [256, 2048], P('ep')
- new_state: float32 [256, 16, 64, 64], P('ep', 'tp')
Inputs may be any that keep to these rules, and one draw needn't show every extreme that they name: `routes`: each row names 6 different experts. In the rows of one device (aligned blocks of 16 rows) no expert is named more than 8 times, and in every draw some expert is named exactly 8 times in some block.
All inputs are finite; a program needn't handle non-finite values.
Results may differ from a plain program's by a relative error of at most 0.02.
Values may be sent and summed in bfloat16 or wider, within the bound.
A program may use at most 128 MiB of HBM per device.

v0:
```python
import jax
import jax.numpy as jnp
from jax import lax
from jax.sharding import PartitionSpec as P

HEAD = 64
HEADS = 16
EPS = 1e-06
THETA = 10000.0


def rounded(values):
    return lax.optimization_barrier(values.astype(jnp.bfloat16)).astype(jnp.float32)


def scaled_rows(values, gain_row):
    widened = values.astype(jnp.float32)
    return widened * lax.rsqrt(jnp.mean(widened * widened, axis=-1, keepdims=True) + EPS) * gain_row


def rotate(vectors, lengths):
    half_dim = vectors.shape[-1] // 2
    frequency = THETA ** (-jnp.arange(half_dim, dtype=jnp.float32) / half_dim)
    angles = lengths.astype(jnp.float32)[:, None] * frequency[None, :]
    cosine = jnp.cos(angles)[:, None, :]
    sine_part = jnp.sin(angles)[:, None, :]
    leading = vectors[..., :half_dim]
    trailing = vectors[..., half_dim:]
    return jnp.concatenate(
        [leading * cosine - trailing * sine_part, trailing * cosine + leading * sine_part], axis=-1
    )


def decay_table(head_count):
    head_order = jnp.arange(head_count, dtype=jnp.float32)
    return 1.0 - jnp.exp2(-5.0 - 7.0 * head_order / (head_count - 1))


def retain(queries, keys_new, values, out_gate, prior_state, lengths, decays):
    seq_count = queries.shape[0]
    head_count = decays.shape[0]
    layout = (seq_count, head_count, HEAD)
    rot_query = rotate(queries.astype(jnp.float32).reshape(layout), lengths)
    rot_key = rotate(keys_new.astype(jnp.float32).reshape(layout), lengths) * HEAD ** (-0.5)
    wide_values = values.astype(jnp.float32).reshape(layout)
    from_state = jnp.einsum(
        "shd,shde->she", rot_query, prior_state, precision=lax.Precision.HIGHEST
    )
    self_term = jnp.sum(rot_query * rot_key, axis=-1, keepdims=True)
    read_out = decays[None, :, None] * from_state + self_term * wide_values
    new_state = (
        decays[None, :, None, None] * prior_state
        + rot_key[..., :, None] * wide_values[..., None, :]
    )
    normed = read_out * lax.rsqrt(jnp.mean(read_out * read_out, axis=-1, keepdims=True) + EPS)
    gated_rows = normed.reshape(seq_count, head_count * HEAD) * jax.nn.silu(
        out_gate.astype(jnp.float32)
    )
    return (gated_rows.astype(jnp.bfloat16), new_state)


def on_device(
    tokens,
    lengths,
    prior_state,
    mix_gain,
    post_gain,
    ffn_gain,
    out_gain,
    query_weight,
    key_weight,
    value_weight,
    gate_weight,
    out_weight,
    routes,
    route_gates,
    expert_gate,
    expert_up,
    expert_down,
    shared_gate,
    shared_up,
    shared_down,
):
    seq_here = tokens.shape[0]
    model_width = tokens.shape[1]
    local_cols = query_weight.shape[1]
    normed = scaled_rows(tokens, mix_gain).astype(jnp.bfloat16)
    features = lax.all_to_all(normed, "ep", split_axis=1, concat_axis=0, tiled=True)
    joined = jnp.concatenate((query_weight, key_weight, value_weight, gate_weight), axis=1)
    summed = lax.psum_scatter(
        jnp.dot(features, joined, preferred_element_type=jnp.float32),
        "ep",
        scatter_dimension=0,
        tiled=True,
    )
    projected = tuple((summed[:, role * local_cols : (role + 1) * local_cols] for role in range(4)))
    queries, keys_new, values, out_gate = tuple(
        (member.astype(jnp.bfloat16) for member in projected)
    )
    heads_here = local_cols // HEAD
    decays = lax.dynamic_slice_in_dim(
        decay_table(HEADS), lax.axis_index("tp") * heads_here, heads_here, 0
    )
    retained, new_state = retain(queries, keys_new, values, out_gate, prior_state, lengths, decays)
    column_part = jnp.dot(
        lax.all_gather(retained, "ep", axis=0, tiled=True),
        out_weight,
        preferred_element_type=jnp.float32,
    ).astype(jnp.bfloat16)
    partial_mix = lax.all_to_all(column_part, "ep", split_axis=0, concat_axis=1, tiled=True).astype(
        jnp.float32
    )
    mixed_sum = rounded(
        lax.psum(rounded(partial_mix).astype(jnp.bfloat16), "tp").astype(jnp.float32)
    )
    middle = rounded(tokens.astype(jnp.float32) + scaled_rows(mixed_sum, post_gain))
    moe_in = scaled_rows(middle, ffn_gain).astype(jnp.bfloat16)
    experts_all = lax.axis_size("ep")
    topk_here = routes.shape[1]
    capacity = seq_here * topk_here // experts_all + 2
    slot_count = experts_all * capacity
    flat_routes = routes.reshape(-1)
    onehot = (flat_routes[:, None] == jnp.arange(experts_all, dtype=jnp.int32)[None, :]).astype(
        jnp.int32
    )
    earlier = jnp.cumsum(onehot, axis=0) - onehot
    ranks = jnp.sum(earlier * onehot, axis=1)
    slot_ids = flat_routes * capacity + ranks
    placing = (jnp.arange(slot_count, dtype=jnp.int32)[:, None] == slot_ids[None, :]).reshape(
        slot_count, seq_here, topk_here
    )
    dispatch_rows = jnp.any(placing, axis=2).astype(jnp.bfloat16)
    combine = jnp.sum(
        jnp.where(placing, route_gates[None, :, :], jnp.zeros((), jnp.float32)), axis=2
    ).T
    outgoing = jnp.dot(dispatch_rows, moe_in, preferred_element_type=jnp.float32).astype(
        jnp.bfloat16
    )
    outgoing = outgoing.reshape(experts_all, capacity, model_width)
    gate_local = expert_gate[0]
    up_local = expert_up[0]
    down_local = expert_down[0]
    arrived = lax.all_to_all(outgoing, "ep", split_axis=0, concat_axis=0, tiled=True)
    sources = arrived.shape[0]
    held_slots = arrived.shape[1]
    flat_in = arrived.reshape(sources * held_slots, model_width)
    hidden = (
        jax.nn.silu(jnp.dot(flat_in, gate_local, preferred_element_type=jnp.float32))
        * jnp.dot(flat_in, up_local, preferred_element_type=jnp.float32)
    ).astype(jnp.bfloat16)
    partial_out = rounded(jnp.dot(hidden, down_local, preferred_element_type=jnp.float32))
    expert_sum = lax.psum(partial_out.astype(jnp.bfloat16), "tp")
    returned = lax.all_to_all(
        expert_sum.reshape(sources, held_slots, -1), "ep", split_axis=0, concat_axis=0, tiled=True
    )
    back_rows = returned.reshape(slot_count, -1).astype(jnp.float32)
    routed = jnp.dot(combine, back_rows, precision=lax.Precision.HIGHEST)
    shared_hidden = (
        jax.nn.silu(jnp.dot(moe_in, shared_gate, preferred_element_type=jnp.float32))
        * jnp.dot(moe_in, shared_up, preferred_element_type=jnp.float32)
    ).astype(jnp.bfloat16)
    shared_part = rounded(jnp.dot(shared_hidden, shared_down, preferred_element_type=jnp.float32))
    shared_out = lax.psum(shared_part.astype(jnp.bfloat16), "tp")
    mixture = shared_out.astype(jnp.float32) + routed
    result = (middle + scaled_rows(mixture, out_gain)).astype(jnp.bfloat16)
    return (result, new_state)


def solution(mesh):
    return jax.shard_map(
        on_device,
        mesh=mesh,
        in_specs=(
            P("ep", None),
            P("ep"),
            P("ep", "tp", None, None),
            P(),
            P(),
            P(),
            P(),
            P("ep", "tp"),
            P("ep", "tp"),
            P("ep", "tp"),
            P("ep", "tp"),
            P("tp", "ep"),
            P("ep", None),
            P("ep", None),
            P("ep", None, "tp"),
            P("ep", None, "tp"),
            P("ep", "tp", None),
            P(None, "tp"),
            P(None, "tp"),
            P("tp", None),
        ),
        out_specs=(P("ep", None), P("ep", "tp", None, None)),
        check_vma=False,
    )
```

profile of v0, /device:TPU:0, one launch (start us, length us, event | category | flops | bytes accessed | tf_op | source)
XLA Modules:
  0.0 254.3 jit_solution(6704595756294250518)
XLA Ops:
  7.2 0.0 copy-start
  7.2 0.0 copy-start.10
  7.2 0.0 reduce-scatter.2.cloned.1.call-start
  7.2 1.0 fusion.25
  8.3 0.9 copy_bitcast_fusion.1
  9.2 15.7 %all_to_all.48 = bf16[16,16,128]{2,0,1:T(8,128)(2,1)S(1)} all-to-all(bf16[16,16,128]{2,0,1:T(8,128)(2,1)S(1)} %copy_bitcast_fusion.1), channel_id=1, replica_groups=mesh['ep'=16,'tp'=2] {'ep'}, dimensions={1} | all-to-all | bytes 131072 | tf_op jit(solution)/shard_map/all_to_all | solution.py:88
  24.9 2.8 %fusion.11 = f32[256,2048]{1,0:T(8,128)} fusion(bf16[256,128]{1,0:T(8,128)(2,1)S(1)} %bitcast.57, bf16[128,512]{1,0:T(8,128)(2,1)} %param.30, bf16[128,512]{1,0:T(8,128)(2,1)} %param.29, bf16[128,512]{1,0:T(8,128)(2,1)} %param.28, bf16[128,512]{1,0:T(8,128)(2,1)} %param.27), kind=kOutput, calls=%fused_computation.18 | convolution fusion | flops 136314880 | bytes 2686976 | tf_op jit(solution)/shard_map/dot_general | solution.py:91
  27.7 0.0 reduce-scatter.2.cloned.1.call-update
  27.8 0.0 copy-start.2
  27.8 0.0 copy-start.7
  27.8 0.0 copy-start.4
  27.8 0.1 copy.38
  27.9 0.1 eq.30
  28.0 0.1 fusion.40
  28.1 0.1 reduce_window_sum.11
  28.2 0.2 select_reduce_fusion.1
  28.4 0.1 reduce_sum.80
  28.5 0.1 copy.39
  28.6 0.1 dynamic_slice.3
  28.7 0.1 multiply_cosine_fusion
  28.8 77.1 %reduce-scatter.2.cloned.1.call-done = f32[16,2048]{1,0:T(8,128)} async-done(((f32[256,2048]{1,0:T(8,128)}), f32[16,2048]{1,0:T(8,128)}) %reduce-scatter.2.cloned.1.call-update) | async-done | bytes 131088 | tf_op jit(solution)/shard_map/reduce_scatter | solution.py:90
  105.9 0.9 convert.9
  106.8 0.1 reshape.191
  106.9 0.1 reshape.193
  107.0 0.1 reshape.189
  107.1 0.1 multiply_subtract_fusion
  107.2 0.1 pad_maximum_fusion
  107.3 5.3 %fusion.62 = f32[16,8,1,64]{3,2,1,0:T(1,128)S(1)} fusion(f32[16,8,64,1]{2,3,1,0:T(1,128)S(1)} %bitcast.55, f32[16,8,64,64]{3,2,1,0:T(8,128)} %param.22), kind=kOutput, calls=%fused_computation.103 | convolution fusion | flops 6291456 | bytes 2162688 | tf_op jit(solution)/shard_map/shd,shde->she/dot_general | solution.py:46
  112.6 0.2 multiply_reduce_fusion.1
  112.8 0.1 broadcast_multiply_fusion
  112.9 0.0 copy-start.1
  112.9 0.1 reshape.183
  113.0 38.2 %all_gather.3 = bf16[256,512]{1,0:T(8,128)(2,1)S(1)} all-gather(bf16[16,512]{1,0:T(8,128)(2,1)S(1)} %fusion.46), channel_id=1, replica_groups=mesh['ep'=16,'tp'=2] {'ep'}, dimensions={0}, use_global_device_ids=true | all-gather | bytes 278528 | tf_op jit(solution)/shard_map/all_gather | solution.py:106
  151.2 0.0 copy-done.3
  151.2 0.8 convolution_convert_fusion.3
  152.1 3.5 %all-to-all-start.1 = ((bf16[16,16,128]{2,1,0:T(8,128)(2,1)}), bf16[16,16,128]{2,1,0:T(8,128)(2,1)S(1)}, u32[]{:S(2)}, u32[]{:S(2)}) async-start(bf16[16,16,128]{2,1,0:T(8,128)(2,1)} %bitcast.6), calls=%async_computation.2 | async-start | bytes 131072 | tf_op jit(solution)/shard_map/all_to_all | solution.py:110
  155.6 0.0 all-reduce.4.cloned.1.call-start
  155.6 7.4 %all-to-all-done.1 = bf16[16,16,128]{2,1,0:T(8,128)(2,1)S(1)} async-done(((bf16[16,16,128]{2,1,0:T(8,128)(2,1)}), bf16[16,16,128]{2,1,0:T(8,128)(2,1)S(1)}, u32[]{:S(2)}, u32[]{:S(2)}) %all-to-all-start.1) | async-done | bytes 65568 | tf_op jit(solution)/shard_map/all_to_all | solution.py:110
  163.1 0.6 copy_bitcast_fusion
  163.7 0.0 all-reduce.4.cloned.1.call-update
  163.7 0.1 fusion.41
  163.8 14.5 %all-reduce.4.cloned.1.call-done = bf16[16,2048]{1,0:T(8,128)(2,1)} async-done(((bf16[16,2048]{1,0:T(8,128)(2,1)}), bf16[16,2048]{1,0:T(8,128)(2,1)}) %all-reduce.4.cloned.1.call-update) | async-done | bytes 65552 | tf_op jit(solution)/shard_map/psum | solution.py:114
  178.3 1.0 fusion.23
  179.3 0.0 copy-done.2
  179.3 0.9 fusion.28
  180.2 0.1 fusion.29
  180.4 1.1 fusion.1
  181.5 6.8 %all-to-all-start.2 = ((bf16[16,8,2048]{2,1,0:T(8,128)(2,1)}), bf16[16,8,2048]{2,1,0:T(8,128)(2,1)S(1)}, u32[]{:S(2)}, u32[]{:S(2)}) async-start(bf16[16,8,2048]{2,1,0:T(8,128)(2,1)} %fusion.1), calls=%async_computation.3 | async-start | bytes 1048576 | tf_op jit(solution)/shard_map/all_to_all | solution.py:143
  188.4 0.0 all-reduce.6.cloned.1.call-start
  188.4 1.5 fusion.60
  189.9 3.0 %convolution_convert_fusion.2 = bf16[16,2048]{1,0:T(8,128)(2,1)} fusion(bf16[256,2048]{1,0:T(8,128)(2,1)} %param.39, bf16[2048,256]{1,0:T(8,128)(2,1)} %param.38, f32[16,256]{1,0:T(8,128)S(1)} %fusion.60, bf16[16,2048]{1,0:T(8,128)(2,1)S(1)} %fusion.28, f32[2048]{0:T(1024)S(1)} %copy-done.4, f32[16]{0:T(128)S(1)} %add_rsqrt_fusion.2), kind=kOutput, calls=%fused_computation.6 | convolution fusion | flops 33742848 | bytes 2252864 | tf_op jit(solution)/shard_map/dot_general | solution.py:162
  192.9 10.9 %all-to-all-done.2 = bf16[16,8,2048]{2,1,0:T(8,128)(2,1)S(1)} async-done(((bf16[16,8,2048]{2,1,0:T(8,128)(2,1)}), bf16[16,8,2048]{2,1,0:T(8,128)(2,1)S(1)}, u32[]{:S(2)}, u32[]{:S(2)}) %all-to-all-start.2) | async-done | bytes 524320 | tf_op jit(solution)/shard_map/all_to_all | solution.py:143
  203.8 1.5 fusion.9
  205.4 1.6 convolution_convert_fusion
  207.0 0.0 all-reduce.6.cloned.1.call-update
  207.0 17.3 %all-reduce.6.cloned.1.call-done = (bf16[16,8,2048]{2,1,0:T(8,128)(2,1)}, bf16[16,2048]{1,0:T(8,128)(2,1)}) async-done(((bf16[16,8,2048]{2,1,0:T(8,128)(2,1)}, bf16[16,2048]{1,0:T(8,128)(2,1)}), (bf16[16,8,2048]{2,1,0:T(8,128)(2,1)}, bf16[16,2048]{1,0:T(8,128)(2,1)})) %all-reduce.6.cloned.1.call-update) | async-done | bytes 589840 | tf_op jit(solution)/shard_map/psum | solution.py:152
  224.3 6.8 %all-to-all-start.3 = ((bf16[16,8,2048]{2,1,0:T(8,128)(2,1)}), bf16[16,8,2048]{2,1,0:T(8,128)(2,1)S(1)}, u32[]{:S(2)}, u32[]{:S(2)}) async-start(bf16[16,8,2048]{2,1,0:T(8,128)(2,1)} %get-tuple-element.2), calls=%async_computation.4 | async-start | bytes 1048576 | tf_op jit(solution)/shard_map/all_to_all | solution.py:153
  231.1 0.1 select_reduce_fusion
  231.2 0.0 copy-start.5
  231.2 0.0 copy-start.8
  231.2 4.3 %multiply_add_fusion = f32[16,8,64,64]{3,2,1,0:T(8,128)} fusion(f32[16,8,64,64]{3,2,1,0:T(8,128)} %param.22, f32[16,8,64]{2,1,0:T(8,128)S(1)} %reshape.193, f32[16,8,64]{2,1,0:T(8,128)S(1)} %get-tuple-element.20, f32[8]{0:T(128)S(1)} %dynamic_slice.3), kind=kLoop, calls=%fused_computation.1 | loop fusion | flops 1572864 | bytes 4259872 | tf_op jit(solution)/shard_map/add | solution.py:52
  235.5 11.1 %all-to-all-done.3 = bf16[16,8,2048]{2,1,0:T(8,128)(2,1)S(1)} async-done(((bf16[16,8,2048]{2,1,0:T(8,128)(2,1)}), bf16[16,8,2048]{2,1,0:T(8,128)(2,1)S(1)}, u32[]{:S(2)}, u32[]{:S(2)}) %all-to-all-start.3) | async-done | bytes 524320 | tf_op jit(solution)/shard_map/all_to_all | solution.py:153
  246.6 0.4 multiply_reduce_fusion
  247.0 0.7 fusion.32
  (23 shorter events, 0.1 us)
Async XLA Ops:
  7.2 198.2 %copy-start = (bf16[1,256,2048]{2,1,0:T(8,128)(2,1)S(1)}, bf16[1,256,2048]{2,1,0:T(8,128)(2,1)}, u32[]{:S(2)}) copy-start(bf16[1,256,2048]{2,1,0:T(8,128)(2,1)} %param.36) | copy-start | bytes 3145732
  7.2 20.6 %copy-start.10 = (s32[16]{0:T(128)S(1)}, s32[16]{0:T(128)}, u32[]{:S(2)}) copy-start(s32[16]{0:T(128)} %param.21) | copy-start | bytes 196
  7.2 20.6 %copy-start.6 = (s32[16,6]{0,1:T(8,128)S(1)}, s32[16,6]{0,1:T(8,128)}, u32[]{:S(2)}) copy-start(s32[16,6]{0,1:T(8,128)} %param.32) | copy-start | bytes 1156
  7.2 98.7 %reduce-scatter.2.cloned.1.call-start = ((), (), s32[]{:S(2)}) async-start(), calls=%async_computation.5 | async-start | bytes 2228224 | tf_op jit(solution)/shard_map/reduce_scatter | solution.py:90
  27.7 123.5 %copy-start.3 = (bf16[512,128]{1,0:T(8,128)(2,1)S(1)}, bf16[512,128]{1,0:T(8,128)(2,1)}, u32[]{:S(2)}) copy-start(bf16[512,128]{1,0:T(8,128)(2,1)} %param.31) | copy-start | bytes 393220
  27.8 151.5 %copy-start.2 = (bf16[16,2048]{1,0:T(8,128)(2,1)S(1)}, bf16[16,2048]{1,0:T(8,128)(2,1)}, u32[]{:S(2)}) copy-start(bf16[16,2048]{1,0:T(8,128)(2,1)} %param.20) | copy-start | bytes 196612
  27.8 151.5 %copy-start.7 = (f32[2048]{0:T(1024)S(1)}, f32[2048]{0:T(1024)}, u32[]{:S(2)}) copy-start(f32[2048]{0:T(1024)} %param.24) | copy-start | bytes 24580
  27.8 152.6 %copy-start.4 = (f32[2048]{0:T(1024)S(1)}, f32[2048]{0:T(1024)}, u32[]{:S(2)}) copy-start(f32[2048]{0:T(1024)} %param.25) | copy-start | bytes 24580
  112.9 92.5 %copy-start.1 = (bf16[1,2048,256]{2,1,0:T(8,128)(2,1)S(1)}, bf16[1,2048,256]{2,1,0:T(8,128)(2,1)}, u32[]{:S(2)}) copy-start(bf16[1,2048,256]{2,1,0:T(8,128)(2,1)} %param.35) | copy-start | bytes 3145732
  152.1 11.0 %all-to-all-start.1 = ((bf16[16,16,128]{2,1,0:T(8,128)(2,1)}), bf16[16,16,128]{2,1,0:T(8,128)(2,1)S(1)}, u32[]{:S(2)}, u32[]{:S(2)}) async-start(bf16[16,16,128]{2,1,0:T(8,128)(2,1)} %bitcast.6), calls=%async_computation.2 | async-start | bytes 131072 | tf_op jit(solution)/shard_map/all_to_all | solution.py:110
  155.6 22.7 %all-reduce.4.cloned.1.call-start = ((), (), s32[]{:S(2)}) async-start(), calls=%async_computation.6 | async-start | bytes 131072 | tf_op jit(solution)/shard_map/psum | solution.py:114
  181.5 22.3 %all-to-all-start.2 = ((bf16[16,8,2048]{2,1,0:T(8,128)(2,1)}), bf16[16,8,2048]{2,1,0:T(8,128)(2,1)S(1)}, u32[]{:S(2)}, u32[]{:S(2)}) async-start(bf16[16,8,2048]{2,1,0:T(8,128)(2,1)} %fusion.1), calls=%async_computation.3 | async-start | bytes 1048576 | tf_op jit(solution)/shard_map/all_to_all | solution.py:143
  188.4 35.9 %all-reduce.6.cloned.1.call-start = ((), (), s32[]{:S(2)}) async-start(), calls=%async_computation.7 | async-start | bytes 1179648 | tf_op jit(solution)/shard_map/psum | solution.py:152
  189.9 41.2 %copy-start.9 = (f32[16,6]{0,1:T(8,128)S(1)}, f32[16,6]{0,1:T(8,128)}, u32[]{:S(2)}) copy-start(f32[16,6]{0,1:T(8,128)} %param.33) | copy-start | bytes 1156
  224.3 22.3 %all-to-all-start.3 = ((bf16[16,8,2048]{2,1,0:T(8,128)(2,1)}), bf16[16,8,2048]{2,1,0:T(8,128)(2,1)S(1)}, u32[]{:S(2)}, u32[]{:S(2)}) async-start(bf16[16,8,2048]{2,1,0:T(8,128)(2,1)} %get-tuple-element.2), calls=%async_computation.4 | async-start | bytes 1048576 | tf_op jit(solution)/shard_map/all_to_all | solution.py:153
  231.2 15.4 %copy-start.5 = (bf16[16,2048]{1,0:T(8,128)(2,1)S(1)}, bf16[16,2048]{1,0:T(8,128)(2,1)}, u32[]{:S(2)}) copy-start(bf16[16,2048]{1,0:T(8,128)(2,1)} %get-tuple-element.3) | copy-start | bytes 196612
  231.2 15.8 %copy-start.8 = (f32[2048]{0:T(1024)S(1)}, f32[2048]{0:T(1024)}, u32[]{:S(2)}) copy-start(f32[2048]{0:T(1024)} %param.26) | copy-start | bytes 24580
Sparse Core Ops, SparseCore 0:
  27.9 77.9 reduce-scatter.1
  163.9 14.3 all-reduce.3
  207.1 17.0 all-reduce.5
where the time goes:
time: 255 us; the launch traced here: 254 us
  waiting for transfers between devices  138 us (54%)
  blocking collectives  53.9 us (21%)
  matrix products  18.1 us (7%)
  starting transfers between devices  17.3 us (7%)
  between operations  14.1 us (6%)
  other arithmetic  11.2 us (4%)
    reduce_scatter x1, waiting for transfers between devices, on_device(): lax.psum_scatter(jnp.dot(features, joined, preferred_element_type=jnp.flo...  77.1 us
    all_gather x1, blocking collectives, on_device(): lax.all_gather(retained, 'ep', axis=0, tiled=True)  38.2 us
    psum x1, waiting for transfers between devices, on_device(): expert_sum = lax.psum(partial_out.astype(jnp.bfloat16), 'tp')  17.3 us
    all_to_all x1, blocking collectives, on_device(): lax.all_to_all(normed, 'ep', split_axis=1, concat_axis=0, tiled=True)  15.7 us
    psum x1, waiting for transfers between devices, on_device(): lax.psum(rounded(partial_mix).astype(jnp.bfloat16), 'tp')  14.5 us
    all_to_all x1, waiting for transfers between devices, on_device(): lax.all_to_all(expert_sum.reshape(sources, held_slots, -1), 'ep', split_a...  11.1 us
    all_to_all x1, waiting for transfers between devices, on_device(): lax.all_to_all(outgoing, 'ep', split_axis=0, concat_axis=0, tiled=True)  10.9 us
    all_to_all x1, waiting for transfers between devices, on_device(): lax.all_to_all(column_part, 'ep', split_axis=0, concat_axis=1, tiled=True)  7.44 us
  transfers between devices with their start and end apart: 6, of which 6 were waited for; matrix products, arithmetic and copies ran while one was open for 4% of the time, Pallas kernels for 0%

commit v1 on v0

--- a/solution.py
+++ b/solution.py
@@ -111,7 +111,9 @@
         jnp.float32
     )
     mixed_sum = rounded(
-        lax.psum(rounded(partial_mix).astype(jnp.bfloat16), "tp").astype(jnp.float32)
+        jnp.sum(lax.all_gather(rounded(partial_mix).astype(jnp.bfloat16), "tp"), axis=0).astype(
+            jnp.float32
+        )
     )
     middle = rounded(tokens.astype(jnp.float32) + scaled_rows(mixed_sum, post_gain))
     moe_in = scaled_rows(middle, ffn_gain).astype(jnp.bfloat16)

time: 255 us -> 237 us (0.929)
  waiting for transfers between devices: 138 us -> 124 us
  starting transfers between devices: 17.3 us -> 14 us
    psum x1 -> x0, waiting for transfers between devices: 14.5 us -> none  [on_device(): lax.psum(rounded(partial_mix).astype(jnp.bfloat16), 'tp')]
    all_to_all x1, starting transfers between devices: 6.84 us -> 3.57 us  [on_device(): lax.all_to_all(outgoing, 'ep', split_axis=0, concat_axis=0, tiled=True)]
  transfers between devices with their start and end apart: 6 -> 5, of which waited for: 6 -> 5; matrix products, arithmetic and copies ran while one was open for 4% -> 4% of each run, Pallas kernels for 0% -> 0%
where the time goes in v1:
time: 237 us; the launch traced here: 236 us
  waiting for transfers between devices  124 us (52%)
  blocking collectives  55.3 us (23%)
  matrix products  18.1 us (8%)
  between operations  14.4 us (6%)
  starting transfers between devices  14 us (6%)
  other arithmetic  9.55 us (4%)
    reduce_scatter x1, waiting for transfers between devices, on_device(): lax.psum_scatter(jnp.dot(features, joined, preferred_element_type=jnp.flo...  77.4 us
    all_gather x1, blocking collectives, on_device(): lax.all_gather(retained, 'ep', axis=0, tiled=True)  37.8 us
    psum x1, waiting for transfers between devices, on_device(): expert_sum = lax.psum(partial_out.astype(jnp.bfloat16), 'tp')  17.4 us
    all_to_all x1, blocking collectives, on_device(): lax.all_to_all(normed, 'ep', split_axis=1, concat_axis=0, tiled=True)  15.7 us
    all_to_all x1, waiting for transfers between devices, on_device(): lax.all_to_all(expert_sum.reshape(sources, held_slots, -1), 'ep', split_a...  11.1 us
    all_to_all x1, waiting for transfers between devices, on_device(): lax.all_to_all(outgoing, 'ep', split_axis=0, concat_axis=0, tiled=True)  10.9 us
    all_to_all x1, waiting for transfers between devices, on_device(): lax.all_to_all(column_part, 'ep', split_axis=0, concat_axis=1, tiled=True)  7.4 us
    all_to_all x1, starting transfers between devices, on_device(): lax.all_to_all(expert_sum.reshape(sources, held_slots, -1), 'ep', split_a...  6.84 us
  transfers between devices with their start and end apart: 5, of which 5 were waited for; matrix products, arithmetic and copies ran while one was open for 4% of the time, Pallas kernels for 0%

profile of v1, /device:TPU:0, one launch (start us, length us, event | category | flops | bytes accessed | tf_op | source)
XLA Modules:
  0.0 236.3 jit_solution(9570223004432646994)
XLA Ops:
  7.2 0.0 copy-start
  7.2 0.0 copy-start.10
  7.2 0.0 copy-start.6
  7.2 0.0 reduce-scatter.2.cloned.1.call-start
  7.2 1.0 fusion.25
  8.3 0.9 copy_bitcast_fusion.1
  9.2 15.7 %all_to_all.48 = bf16[16,16,128]{2,0,1:T(8,128)(2,1)S(1)} all-to-all(bf16[16,16,128]{2,0,1:T(8,128)(2,1)S(1)} %copy_bitcast_fusion.1), channel_id=1, replica_groups=mesh['ep'=16,'tp'=2] {'ep'}, dimensions={1} | all-to-all | bytes 131072 | tf_op jit(solution)/shard_map/all_to_all | solution.py:88
  24.9 2.8 %fusion.11 = f32[256,2048]{1,0:T(8,128)} fusion(bf16[256,128]{1,0:T(8,128)(2,1)S(1)} %bitcast.59, bf16[128,512]{1,0:T(8,128)(2,1)} %param.30, bf16[128,512]{1,0:T(8,128)(2,1)} %param.29, bf16[128,512]{1,0:T(8,128)(2,1)} %param.28, bf16[128,512]{1,0:T(8,128)(2,1)} %param.27), kind=kOutput, calls=%fused_computation.18 | convolution fusion | flops 136314880 | bytes 2686976 | tf_op jit(solution)/shard_map/dot_general | solution.py:91
  27.7 0.0 reduce-scatter.2.cloned.1.call-update
  27.8 0.0 copy-start.2
  27.8 0.0 copy-start.7
  27.8 0.0 copy-done.6
  27.8 0.1 copy.42
  27.9 0.1 eq.30
  28.0 0.1 fusion.40
  28.1 0.1 reduce_window_sum.11
  28.2 0.2 select_reduce_fusion.1
  28.4 0.0 copy-start.4
  28.4 0.1 reduce_sum.93
  28.5 0.1 copy.43
  28.6 0.1 dynamic_slice.3
  28.7 0.1 multiply_cosine_fusion
  28.8 77.4 %reduce-scatter.2.cloned.1.call-done = f32[16,2048]{1,0:T(8,128)} async-done(((f32[256,2048]{1,0:T(8,128)}), f32[16,2048]{1,0:T(8,128)}) %reduce-scatter.2.cloned.1.call-update) | async-done | bytes 131088 | tf_op jit(solution)/shard_map/reduce_scatter | solution.py:90
  106.2 0.9 convert.10
  107.1 0.1 reshape.191
  107.2 0.1 reshape.193
  107.3 0.1 reshape.189
  107.4 0.1 multiply_subtract_fusion
  107.5 0.1 pad_maximum_fusion
  107.6 5.3 %fusion.62 = f32[16,8,1,64]{3,2,1,0:T(1,128)S(1)} fusion(f32[16,8,64,1]{2,3,1,0:T(1,128)S(1)} %bitcast.56, f32[16,8,64,64]{3,2,1,0:T(8,128)} %param.22), kind=kOutput, calls=%fused_computation.103 | convolution fusion | flops 6291456 | bytes 2162688 | tf_op jit(solution)/shard_map/shd,shde->she/dot_general | solution.py:46
  112.9 0.2 multiply_reduce_fusion.1
  113.1 0.1 broadcast_multiply_fusion
  113.2 0.1 reshape.183
  113.3 0.0 copy-start.1
  113.3 37.8 %all_gather.9 = bf16[256,512]{1,0:T(8,128)(2,1)S(1)} all-gather(bf16[16,512]{1,0:T(8,128)(2,1)S(1)} %fusion.46), channel_id=1, replica_groups=mesh['ep'=16,'tp'=2] {'ep'}, dimensions={0}, use_global_device_ids=true | all-gather | bytes 278528 | tf_op jit(solution)/shard_map/all_gather | solution.py:106
  151.1 0.8 convolution_convert_fusion.3
  151.9 3.5 %all-to-all-start.1 = ((bf16[16,16,128]{2,1,0:T(8,128)(2,1)}), bf16[16,16,128]{2,1,0:T(8,128)(2,1)S(1)}, u32[]{:S(2)}, u32[]{:S(2)}) async-start(bf16[16,16,128]{2,1,0:T(8,128)(2,1)} %bitcast.6), calls=%async_computation.2 | async-start | bytes 131072 | tf_op jit(solution)/shard_map/all_to_all | solution.py:110
  155.5 0.1 fusion.41
  155.6 7.4 %all-to-all-done.1 = bf16[16,16,128]{2,1,0:T(8,128)(2,1)S(1)} async-done(((bf16[16,16,128]{2,1,0:T(8,128)(2,1)}), bf16[16,16,128]{2,1,0:T(8,128)(2,1)S(1)}, u32[]{:S(2)}, u32[]{:S(2)}) %all-to-all-start.1) | async-done | bytes 65568 | tf_op jit(solution)/shard_map/all_to_all | solution.py:110
  163.0 1.9 all-gather
  164.9 0.1 fusion.23
  165.0 0.0 copy-done.2
  165.0 0.0 copy-done.7
  165.0 0.1 fusion.28
  165.1 0.1 fusion.29
  165.3 1.1 fusion.1
  166.4 3.6 %all-to-all-start.2 = ((bf16[16,8,2048]{2,1,0:T(8,128)(2,1)}), bf16[16,8,2048]{2,1,0:T(8,128)(2,1)S(1)}, u32[]{:S(2)}, u32[]{:S(2)}) async-start(bf16[16,8,2048]{2,1,0:T(8,128)(2,1)} %fusion.1), calls=%async_computation.3 | async-start | bytes 1048576 | tf_op jit(solution)/shard_map/all_to_all | solution.py:145
  170.0 0.0 all-reduce.3.cloned.1.call-start
  170.1 1.5 fusion.60
  171.6 3.0 %convolution_convert_fusion.2 = bf16[16,2048]{1,0:T(8,128)(2,1)} fusion(bf16[256,2048]{1,0:T(8,128)(2,1)} %param.39, bf16[2048,256]{1,0:T(8,128)(2,1)} %param.38, f32[16,256]{1,0:T(8,128)S(1)} %fusion.60, bf16[16,2048]{1,0:T(8,128)(2,1)S(1)} %fusion.28, f32[2048]{0:T(1024)S(1)} %copy-done.4, f32[16]{0:T(128)S(1)} %add_rsqrt_fusion.2), kind=kOutput, calls=%fused_computation.6 | convolution fusion | flops 33742848 | bytes 2252864 | tf_op jit(solution)/shard_map/dot_general | solution.py:164
  174.5 10.9 %all-to-all-done.2 = bf16[16,8,2048]{2,1,0:T(8,128)(2,1)S(1)} async-done(((bf16[16,8,2048]{2,1,0:T(8,128)(2,1)}), bf16[16,8,2048]{2,1,0:T(8,128)(2,1)S(1)}, u32[]{:S(2)}, u32[]{:S(2)}) %all-to-all-start.2) | async-done | bytes 524320 | tf_op jit(solution)/shard_map/all_to_all | solution.py:145
  185.4 1.5 fusion.9
  187.0 0.0 copy-done
  187.0 0.0 copy-done.1
  187.0 1.6 convolution_convert_fusion
  188.6 0.0 all-reduce.3.cloned.1.call-update
  188.6 17.4 %all-reduce.3.cloned.1.call-done = (bf16[16,8,2048]{2,1,0:T(8,128)(2,1)}, bf16[16,2048]{1,0:T(8,128)(2,1)}) async-done(((bf16[16,8,2048]{2,1,0:T(8,128)(2,1)}, bf16[16,2048]{1,0:T(8,128)(2,1)}), (bf16[16,8,2048]{2,1,0:T(8,128)(2,1)}, bf16[16,2048]{1,0:T(8,128)(2,1)})) %all-reduce.3.cloned.1.call-update) | async-done | bytes 589840 | tf_op jit(solution)/shard_map/psum | solution.py:154
  206.0 6.8 %all-to-all-start.3 = ((bf16[16,8,2048]{2,1,0:T(8,128)(2,1)}), bf16[16,8,2048]{2,1,0:T(8,128)(2,1)S(1)}, u32[]{:S(2)}, u32[]{:S(2)}) async-start(bf16[16,8,2048]{2,1,0:T(8,128)(2,1)} %get-tuple-element.2), calls=%async_computation.4 | async-start | bytes 1048576 | tf_op jit(solution)/shard_map/all_to_all | solution.py:155
  212.8 0.1 select_reduce_fusion
  213.0 0.0 copy-start.8
  213.0 4.3 %multiply_add_fusion = f32[16,8,64,64]{3,2,1,0:T(8,128)} fusion(f32[16,8,64,64]{3,2,1,0:T(8,128)} %param.22, f32[16,8,64]{2,1,0:T(8,128)S(1)} %reshape.193, f32[16,8,64]{2,1,0:T(8,128)S(1)} %get-tuple-element.20, f32[8]{0:T(128)S(1)} %dynamic_slice.3), kind=kLoop, calls=%fused_computation.1 | loop fusion | flops 1572864 | bytes 4259872 | tf_op jit(solution)/shard_map/add | solution.py:52
  217.3 11.1 %all-to-all-done.3 = bf16[16,8,2048]{2,1,0:T(8,128)(2,1)S(1)} async-done(((bf16[16,8,2048]{2,1,0:T(8,128)(2,1)}), bf16[16,8,2048]{2,1,0:T(8,128)(2,1)S(1)}, u32[]{:S(2)}, u32[]{:S(2)}) %all-to-all-start.3) | async-done | bytes 524320 | tf_op jit(solution)/shard_map/all_to_all | solution.py:155
  228.3 0.4 multiply_reduce_fusion
  228.8 0.7 fusion.32
  (22 shorter events, 0.1 us)
Async XLA Ops:
  7.2 179.8 %copy-start = (bf16[1,256,2048]{2,1,0:T(8,128)(2,1)S(1)}, bf16[1,256,2048]{2,1,0:T(8,128)(2,1)}, u32[]{:S(2)}) copy-start(bf16[1,256,2048]{2,1,0:T(8,128)(2,1)} %param.36) | copy-start | bytes 3145732
  7.2 20.6 %copy-start.10 = (s32[16]{0:T(128)S(1)}, s32[16]{0:T(128)}, u32[]{:S(2)}) copy-start(s32[16]{0:T(128)} %param.21) | copy-start | bytes 196
  7.2 20.6 %copy-start.6 = (s32[16,6]{0,1:T(8,128)S(1)}, s32[16,6]{0,1:T(8,128)}, u32[]{:S(2)}) copy-start(s32[16,6]{0,1:T(8,128)} %param.32) | copy-start | bytes 1156
  7.2 99.0 %reduce-scatter.2.cloned.1.call-start = ((), (), s32[]{:S(2)}) async-start(), calls=%async_computation.5 | async-start | bytes 2228224 | tf_op jit(solution)/shard_map/reduce_scatter | solution.py:90
  27.7 123.4 %copy-start.3 = (bf16[512,128]{1,0:T(8,128)(2,1)S(1)}, bf16[512,128]{1,0:T(8,128)(2,1)}, u32[]{:S(2)}) copy-start(bf16[512,128]{1,0:T(8,128)(2,1)} %param.31) | copy-start | bytes 393220
  27.8 137.2 %copy-start.2 = (bf16[16,2048]{1,0:T(8,128)(2,1)S(1)}, bf16[16,2048]{1,0:T(8,128)(2,1)}, u32[]{:S(2)}) copy-start(bf16[16,2048]{1,0:T(8,128)(2,1)} %param.20) | copy-start | bytes 196612
  27.8 137.2 %copy-start.7 = (f32[2048]{0:T(1024)S(1)}, f32[2048]{0:T(1024)}, u32[]{:S(2)}) copy-start(f32[2048]{0:T(1024)} %param.24) | copy-start | bytes 24580
  28.4 136.9 %copy-start.4 = (f32[2048]{0:T(1024)S(1)}, f32[2048]{0:T(1024)}, u32[]{:S(2)}) copy-start(f32[2048]{0:T(1024)} %param.25) | copy-start | bytes 24580
  113.3 73.7 %copy-start.1 = (bf16[1,2048,256]{2,1,0:T(8,128)(2,1)S(1)}, bf16[1,2048,256]{2,1,0:T(8,128)(2,1)}, u32[]{:S(2)}) copy-start(bf16[1,2048,256]{2,1,0:T(8,128)(2,1)} %param.35) | copy-start | bytes 3145732
  151.9 11.0 %all-to-all-start.1 = ((bf16[16,16,128]{2,1,0:T(8,128)(2,1)}), bf16[16,16,128]{2,1,0:T(8,128)(2,1)S(1)}, u32[]{:S(2)}, u32[]{:S(2)}) async-start(bf16[16,16,128]{2,1,0:T(8,128)(2,1)} %bitcast.6), calls=%async_computation.2 | async-start | bytes 131072 | tf_op jit(solution)/shard_map/all_to_all | solution.py:110
  166.4 19.0 %all-to-all-start.2 = ((bf16[16,8,2048]{2,1,0:T(8,128)(2,1)}), bf16[16,8,2048]{2,1,0:T(8,128)(2,1)S(1)}, u32[]{:S(2)}, u32[]{:S(2)}) async-start(bf16[16,8,2048]{2,1,0:T(8,128)(2,1)} %fusion.1), calls=%async_computation.3 | async-start | bytes 1048576 | tf_op jit(solution)/shard_map/all_to_all | solution.py:145
  170.0 36.0 %all-reduce.3.cloned.1.call-start = ((), (), s32[]{:S(2)}) async-start(), calls=%async_computation.6 | async-start | bytes 1179648 | tf_op jit(solution)/shard_map/psum | solution.py:154
  171.6 41.3 %copy-start.9 = (f32[16,6]{0,1:T(8,128)S(1)}, f32[16,6]{0,1:T(8,128)}, u32[]{:S(2)}) copy-start(f32[16,6]{0,1:T(8,128)} %param.33) | copy-start | bytes 1156
  206.0 22.3 %all-to-all-start.3 = ((bf16[16,8,2048]{2,1,0:T(8,128)(2,1)}), bf16[16,8,2048]{2,1,0:T(8,128)(2,1)S(1)}, u32[]{:S(2)}, u32[]{:S(2)}) async-start(bf16[16,8,2048]{2,1,0:T(8,128)(2,1)} %get-tuple-element.2), calls=%async_computation.4 | async-start | bytes 1048576 | tf_op jit(solution)/shard_map/all_to_all | solution.py:155
  212.9 15.4 %copy-start.5 = (bf16[16,2048]{1,0:T(8,128)(2,1)S(1)}, bf16[16,2048]{1,0:T(8,128)(2,1)}, u32[]{:S(2)}) copy-start(bf16[16,2048]{1,0:T(8,128)(2,1)} %get-tuple-element.3) | copy-start | bytes 196612
  213.0 15.8 %copy-start.8 = (f32[2048]{0:T(1024)S(1)}, f32[2048]{0:T(1024)}, u32[]{:S(2)}) copy-start(f32[2048]{0:T(1024)} %param.26) | copy-start | bytes 24580
Sparse Core Ops, SparseCore 0:
  27.9 78.2 reduce-scatter.1
  188.7 17.2 all-reduce.2
